TPU v7x, 32 devices: a whole 2x2x4 slice. The times are simulated.
32 devices in a mesh: sp: 8 (over z, core), tp: 4 (over y, x).
Axes of the slice: x: 2, y: 2, z: 4, core: 2. Of those that a mesh axis runs over, the one named last changes fastest.
Arguments:
- query_rows: bfloat16 [2048, 2048], P('sp', 'tp'), may hold values from -1000 to 1000
- key_rows: bfloat16 [2048, 256], P('sp'), may hold values from -6 to 6
- value_rows: bfloat16 [2048, 256], P('sp'), may hold values from -6 to 6
- sink_logits: float32 [32], P('tp'), may hold values from 1 to 6
- out_weight: bfloat16 [2048, 2048], P('tp'), may hold values from -0.375 to 0.375
- stream_in: bfloat16 [2048, 2048], P('sp'), may hold values from -6 to 6
- norm_gain: float32 [2048], replicated, may hold values from 0.1 to 1.9
- routes: int32 [2048, 2], P('sp'), may hold values from 0 to 7, all different within a row; in each aligned block of 256 rows (0 to 255, 256 to 511, ...) at most 96 rows name the same one
- route_weights: float32 [2048, 2], P('sp'), may hold values from 0.2 to 1
- gate_weight: bfloat16 [8, 2048, 4096], P('sp', None, 'tp'), may hold values from -0.125 to 0.125
- up_weight: bfloat16 [8, 2048, 4096], P('sp', None, 'tp'), may hold values from -0.125 to 0.125
- down_weight: bfloat16 [8, 4096, 2048], P('sp', 'tp'), may hold values from -0.09375 to 0.09375
Outputs:
- layer_out: bfloat16 [2048, 2048], P(('sp', 'tp'))
Inputs may be any that keep to these rules, and one draw needn't show every extreme that they name: `routes`: each row names 2 different experts. Within the rows of one device (256 aligned rows) no expert is named more than 96 times, a bound that some block reaches.
All inputs are finite; a program needn't handle non-finite values.
Results may differ from a plain program's by a relative error of at most 0.015.
Values may be sent and summed in bfloat16 or wider, within the bound.
A program may use at most 64 MiB of HBM per device.

v0:
```python
import jax
import jax.numpy as jnp
from jax import lax
from jax.sharding import PartitionSpec as P

HEAD_DIM = 64
REP = 8
WINDOW = 128
norm_eps = 1e-06


def shifted(block, axis, distance):
    devices = range(lax.axis_size(axis))
    route = [(i - distance, i) for i in devices if i - distance in devices]
    return lax.ppermute(block, axis, route)


def rms_scale(stream, norm_gain):
    values = stream.astype(jnp.float32)
    scaled = values * lax.rsqrt(jnp.mean(values * values, axis=-1, keepdims=True) + norm_eps)
    return (scaled * norm_gain).astype(jnp.bfloat16)


def slot_tables(routes, experts_n, slot_cap):
    flat_ids = routes.reshape(-1)
    onehot = (flat_ids[:, None] == jnp.arange(experts_n, dtype=jnp.int32)[None, :]).astype(
        jnp.int32
    )
    before = jnp.cumsum(onehot, axis=0) - onehot
    targets = flat_ids * slot_cap + jnp.sum(before * onehot, axis=1)
    pair_token = jnp.arange(flat_ids.shape[0], dtype=jnp.int32) // routes.shape[1]
    slot_token = jnp.zeros((experts_n * slot_cap,), jnp.int32).at[targets].set(pair_token)
    slot_live = jnp.zeros((experts_n * slot_cap,), jnp.int32).at[targets].set(1)
    return (targets, slot_token, slot_live)


def per_device(
    query_rows,
    key_rows,
    value_rows,
    sink_logits,
    out_weight,
    stream_in,
    norm_gain,
    routes,
    route_weights,
    gate_weight,
    up_weight,
    down_weight,
):
    tok_count = query_rows.shape[0]
    local_heads = query_rows.shape[1] // HEAD_DIM
    tp_index = lax.axis_index("tp")
    kv_group = tp_index * local_heads // REP
    own_keys = lax.dynamic_slice_in_dim(key_rows, kv_group * HEAD_DIM, HEAD_DIM, 1)
    own_values = lax.dynamic_slice_in_dim(value_rows, kv_group * HEAD_DIM, HEAD_DIM, 1)
    prior_keys, prior_values = shifted(
        (own_keys[tok_count - WINDOW :], own_values[tok_count - WINDOW :]), "sp", 1
    )
    key_block = jnp.concatenate([prior_keys, own_keys], axis=0)
    value_block = jnp.concatenate([prior_values, own_values], axis=0)
    offset = lax.axis_index("sp") * tok_count
    query_pos = offset + jnp.arange(tok_count, dtype=jnp.int32)
    key_pos = offset - WINDOW + jnp.arange(tok_count + WINDOW, dtype=jnp.int32)
    distance = query_pos[:, None] - key_pos[None, :]
    allowed = (distance >= 0) & (distance < WINDOW) & (key_pos >= 0)[None, :]
    queries = query_rows.reshape(tok_count, local_heads, HEAD_DIM)
    scores = jnp.einsum(
        "qhd,kd->hqk", queries, key_block, preferred_element_type=jnp.float32
    ) * HEAD_DIM ** (-0.5)
    scores = jnp.where(allowed[None], scores, -1e30)
    sink_col = sink_logits.reshape(local_heads, 1, 1)
    row_peak = jnp.maximum(jnp.max(scores, axis=-1, keepdims=True), sink_col)
    exp_terms = jnp.exp(scores - row_peak)
    denom_sum = jnp.sum(exp_terms, axis=-1, keepdims=True) + jnp.exp(sink_col - row_peak)
    attn_probs = (exp_terms / denom_sum).astype(jnp.bfloat16)
    attended = jnp.einsum(
        "hqk,kd->qhd", attn_probs, value_block, preferred_element_type=jnp.float32
    )
    attended = attended.astype(jnp.bfloat16).reshape(tok_count, local_heads * HEAD_DIM)
    row_share = tok_count // lax.axis_size("tp")
    projected = lax.psum(
        jnp.dot(attended, out_weight, preferred_element_type=jnp.float32).astype(jnp.bfloat16), "tp"
    ).astype(jnp.float32)
    stream = (stream_in.astype(jnp.float32) + projected).astype(jnp.bfloat16)
    normed_all = rms_scale(stream, norm_gain)
    own_stream = lax.dynamic_slice_in_dim(stream, tp_index * row_share, row_share, 0)
    experts_n = lax.axis_size("sp")
    top_count = routes.shape[1]
    slot_cap = 3 * tok_count * top_count // (2 * experts_n)
    targets, slot_token, slot_live = slot_tables(routes, experts_n, slot_cap)
    width_share = normed_all.shape[1] // lax.axis_size("tp")
    columns = lax.dynamic_slice_in_dim(normed_all, tp_index * width_share, width_share, 1)
    outgoing = jnp.where(slot_live[:, None] > 0, columns[slot_token], jnp.zeros((), jnp.bfloat16))
    outgoing = outgoing.reshape(experts_n, slot_cap, width_share)
    arrived = lax.all_to_all(outgoing, "sp", split_axis=0, concat_axis=0, tiled=True)
    arrived = lax.all_gather(arrived, "tp", axis=2, tiled=True)
    sources = arrived.shape[0]
    item_count = arrived.shape[1]
    flat_rows = arrived.reshape(sources * item_count, arrived.shape[2])
    gate_act = jnp.dot(flat_rows, gate_weight[0], preferred_element_type=jnp.float32)
    up_act = jnp.dot(flat_rows, up_weight[0], preferred_element_type=jnp.float32)
    hidden = (jax.nn.silu(gate_act) * up_act).astype(jnp.bfloat16)
    partial_value = jnp.dot(hidden, down_weight[0], preferred_element_type=jnp.float32).astype(
        jnp.bfloat16
    )
    partial_value = partial_value.reshape(sources, item_count, partial_value.shape[1])
    returned = lax.all_to_all(partial_value, "sp", split_axis=0, concat_axis=0, tiled=True)
    returned_flat = returned.reshape(experts_n * slot_cap, returned.shape[2])
    pair_weights = route_weights.reshape(-1)
    chosen = returned_flat[targets].astype(jnp.float32) * pair_weights[:, None]
    moe_rows = lax.psum_scatter(
        jnp.sum(
            chosen.reshape(row_share * lax.axis_size("tp"), top_count, chosen.shape[1]), axis=1
        ).astype(jnp.bfloat16),
        "tp",
        scatter_dimension=0,
        tiled=True,
    ).astype(jnp.float32)
    return (own_stream.astype(jnp.float32) + moe_rows).astype(jnp.bfloat16)


def solution(mesh):
    return jax.shard_map(
        per_device,
        mesh=mesh,
        in_specs=(
            P("sp", "tp"),
            P("sp", None),
            P("sp", None),
            P("tp"),
            P("tp", None),
            P("sp", None),
            P(),
            P("sp", None),
            P("sp", None),
            P("sp", None, "tp"),
            P("sp", None, "tp"),
            P("sp", "tp", None),
        ),
        out_specs=P(("sp", "tp"), None),
        check_vma=False,
    )
```

profile of v0, /device:TPU:0, one launch (start us, length us, event | category | flops | bytes accessed | tf_op | source)
XLA Modules:
  0.0 299.9 jit_solution(17080001785737628045)
XLA Ops:
  6.5 0.0 copy-start
  6.5 0.0 copy-start.2
  6.5 0.0 all-reduce.2.cloned.1.call-start
  6.5 1.1 constant_dynamic-slice_fusion
  7.6 0.1 copy.28
  7.7 2.4 collective-permute-start.1
  10.1 0.9 constant_dynamic-slice_fusion.1
  11.1 0.1 copy.27
  11.2 4.6 %collective-permute-start = (bf16[128,64]{0,1:T(8,128)(2,1)S(1)}, bf16[128,64]{0,1:T(8,128)(2,1)S(1)}, u32[]{:S(2)}, u32[]{:S(2)}) collective-permute-start(bf16[128,64]{0,1:T(8,128)(2,1)S(1)} %slice.20), channel_id=1, source_target_pairs={{0,4},{4,8},{8,12},{12,16},{16,20},{20,24},{24,28},{1,5},{5,9},{9,... | collective-permute-start | bytes 49160 | tf_op jit(solution)/shard_map/ppermute | solution.py:15
  15.8 0.8 copy.23
  16.6 0.1 eq.29
  16.8 0.2 fusion.18
  17.0 0.7 broadcast_multiply_fusion
  17.7 1.1 copy.20
  18.8 1.1 reduce-window.6
  19.9 0.0 collective-permute-done.1
  19.9 0.7 fusion.10
  20.6 0.0 copy-done.2
  20.6 0.1 broadcast_maximum_fusion
  20.7 0.7 fusion.9
  21.3 0.1 exponential_add_fusion
  21.4 0.0 collective-permute-done
  21.4 1.0 fusion.14
  22.4 0.0 copy-done
  22.4 1.8 convolution_convert_fusion
  24.2 0.0 all-reduce.2.cloned.1.call-update
  24.2 0.0 all-gather.2.cloned.1.call-start
  24.2 0.2 slice_reduce_fusion
  24.5 0.1 eq.25
  24.6 0.1 copy.22
  24.8 0.1 mul.88
  24.9 0.1 fusion.25
  25.0 2.4 scatter_custom_fusion.1
  27.5 2.4 scatter_custom_fusion
  30.0 0.1 broadcast_in_dim.48
  30.1 0.8 dynamic-slice
  30.8 46.2 %all-reduce.2.cloned.1.call-done = bf16[256,2048]{1,0:T(8,128)(2,1)} async-done(((bf16[256,2048]{1,0:T(8,128)(2,1)}), bf16[256,2048]{1,0:T(8,128)(2,1)}) %all-reduce.2.cloned.1.call-update) | async-done | bytes 1048592 | tf_op jit(solution)/shard_map/psum | solution.py:82
  77.0 2.0 multiply_reduce_fusion.1
  79.1 0.2 convert_element_type.69
  79.3 0.1 fusion.16
  79.5 3.3 %gather_fusion = bf16[768,512]{1,0:T(8,128)(2,1)} fusion(bf16[256,512]{1,0:T(8,128)(2,1)S(1)} %fusion.16, s32[1024]{0:T(1024)S(1)} %pad_clamp_fusion.1), kind=kCustom, calls=%fused_computation | custom fusion | bytes 1575936 | tf_op jit(solution)/shard_map/gather | solution.py:94
  82.8 1.3 broadcast_select_fusion
  84.1 25.5 %all_to_all.10 = bf16[8,96,512]{2,1,0:T(8,128)(2,1)} all-to-all(bf16[8,96,512]{2,1,0:T(8,128)(2,1)S(1)} %broadcast_select_fusion), channel_id=1, replica_groups=mesh['sp'=8,'tp'=4] {'sp'}, dimensions={0} | all-to-all | bytes 1572864 | tf_op jit(solution)/shard_map/all_to_all | solution.py:96
  109.5 0.0 all-gather.2.cloned.1.call-update
  109.6 41.8 %all-gather.2.cloned.1.call-done = bf16[8,96,2048]{2,1,0:T(8,128)(2,1)} async-done(((bf16[8,96,512]{2,1,0:T(8,128)(2,1)}), bf16[8,96,2048]{2,1,0:T(8,128)(2,1)}) %all-gather.2.cloned.1.call-update) | async-done | bytes 3145744 | tf_op jit(solution)/shard_map/all_gather | solution.py:97
  151.4 0.0 copy-start.3
  151.4 6.3 %fusion.2 = f32[768,1024]{1,0:T(8,128)S(1)} fusion(bf16[768,2048]{1,0:T(8,128)(2,1)} %bitcast.64, bf16[1,2048,1024]{2,1,0:T(8,128)(2,1)} %param.22), kind=kOutput, calls=%fused_computation.6 | convolution fusion | flops 3221225472 | bytes 10485760 | tf_op jit(solution)/shard_map/dot_general | solution.py:102
  157.7 0.0 copy-done.3
  157.7 0.0 copy-done.5
  157.7 0.0 copy-start.4
  157.7 3.8 %multiply_convert_fusion = bf16[768,1024]{1,0:T(8,128)(2,1)S(1)} fusion(f32[768,1024]{1,0:T(8,128)S(1)} %fusion.2, bf16[768,2048]{1,0:T(8,128)(2,1)S(1)} %bitcast.65, bf16[1,2048,1024]{2,1,0:T(8,128)(2,1)S(1)} %copy-done.3), kind=kOutput, calls=%fused_computation.13 | convolution fusion | flops 3225944064 | bytes 12058624 | tf_op jit(solution)/shard_map/dot_general | solution.py:101
  161.5 0.0 copy-done.4
  161.5 4.8 %fusion.6 = bf16[768,2048]{1,0:T(8,128)(2,1)} fusion(bf16[768,1024]{1,0:T(8,128)(2,1)S(1)} %multiply_convert_fusion, bf16[1,1024,2048]{2,1,0:T(8,128)(2,1)S(1)} %copy-done.4), kind=kOutput, calls=%fused_computation.11 | convolution fusion | flops 3222798336 | bytes 8912896 | tf_op jit(solution)/shard_map/dot_general | solution.py:104
  166.4 4.7 %all-to-all-start.1 = ((bf16[8,96,2048]{2,1,0:T(8,128)(2,1)}), bf16[8,96,2048]{2,1,0:T(8,128)(2,1)}, u32[]{:S(2)}, u32[]{:S(2)}) async-start(bf16[8,96,2048]{2,1,0:T(8,128)(2,1)} %bitcast.56), calls=%async_computation.1 | async-start | bytes 6291456 | tf_op jit(solution)/shard_map/all_to_all | solution.py:108
  171.1 0.3 reduce-scatter.2.cloned.1.call-start
  171.4 0.0 copy-done.1
  171.4 0.1 copy.25
  171.5 71.2 %all-to-all-done.1 = bf16[8,96,2048]{2,1,0:T(8,128)(2,1)} async-done(((bf16[8,96,2048]{2,1,0:T(8,128)(2,1)}), bf16[8,96,2048]{2,1,0:T(8,128)(2,1)}, u32[]{:S(2)}, u32[]{:S(2)}) %all-to-all-start.1) | async-done | bytes 3145760 | tf_op jit(solution)/shard_map/all_to_all | solution.py:108
  242.7 7.6 %gather_fusion.1 = bf16[512,2048]{1,0:T(8,128)(2,1)} fusion(bf16[768,2048]{1,0:T(8,128)(2,1)} %bitcast.16, s32[1024]{0:T(1024)S(1)} %pad_clamp_fusion), kind=kCustom, calls=%fused_computation.1 | custom fusion | bytes 4196352 | tf_op jit(solution)/shard_map/gather | solution.py:111
  250.3 5.4 %reshape.209 = f32[256,2,2048]{2,1,0:T(2,128)} reshape(bf16[512,2048]{1,0:T(8,128)(2,1)} %gather_fusion.1) | data formatting | bytes 6291456 | tf_op jit(solution)/shard_map/convert_element_type | solution.py:111
  255.7 9.9 %multiply_reduce_fusion = bf16[256,2048]{1,0:T(8,128)(2,1)} fusion(f32[256,2,2048]{2,1,0:T(2,128)} %reshape.209, f32[256,2]{1,0:T(8,128)S(1)} %copy.25), kind=kLoop, calls=%fused_computation.10 | loop fusion | flops 1572864 | bytes 5244928 | tf_op jit(solution)/shard_map/reduce_sum | solution.py:113
  265.6 0.0 reduce-scatter.2.cloned.1.call-update
  265.6 26.0 %reduce-scatter.2.cloned.1.call-done = bf16[64,2048]{1,0:T(8,128)(2,1)} async-done(((bf16[256,2048]{1,0:T(8,128)(2,1)}), bf16[64,2048]{1,0:T(8,128)(2,1)}) %reduce-scatter.2.cloned.1.call-update) | async-done | bytes 262160 | tf_op jit(solution)/shard_map/reduce_scatter | solution.py:112
  291.6 1.7 add_convert_fusion.1
  (18 shorter events, 0.1 us)
Async XLA Ops:
  6.5 15.9 %copy-start = (bf16[512,2048]{1,0:T(8,128)(2,1)S(1)}, bf16[512,2048]{1,0:T(8,128)(2,1)}, u32[]{:S(2)}) copy-start(bf16[512,2048]{1,0:T(8,128)(2,1)} %param.16) | copy-start | bytes 6291460
  6.5 14.0 %copy-start.2 = (f32[8]{0:T(128)S(1)}, f32[8]{0:T(128)}, u32[]{:S(2)}) copy-start(f32[8]{0:T(128)} %param.15) | copy-start | bytes 100
  6.5 70.5 %all-reduce.2.cloned.1.call-start = ((), (), s32[]{:S(2)}) async-start(), calls=%async_computation.3 | async-start | bytes 2097152 | tf_op jit(solution)/shard_map/psum | solution.py:82
  7.7 12.2 %collective-permute-start.1 = (bf16[128,64]{0,1:T(8,128)(2,1)S(1)}, bf16[128,64]{0,1:T(8,128)(2,1)S(1)}, u32[]{:S(2)}, u32[]{:S(2)}) collective-permute-start(bf16[128,64]{0,1:T(8,128)(2,1)S(1)} %slice.21), channel_id=1, source_target_pairs={{0,4},{4,8},{8,12},{12,16},{16,20},{20,24},{24,28},{1,5},{5,9},{9,... | collective-permute-start | bytes 49160 | tf_op jit(solution)/shard_map/ppermute | solution.py:15
  11.2 10.2 %collective-permute-start = (bf16[128,64]{0,1:T(8,128)(2,1)S(1)}, bf16[128,64]{0,1:T(8,128)(2,1)S(1)}, u32[]{:S(2)}, u32[]{:S(2)}) collective-permute-start(bf16[128,64]{0,1:T(8,128)(2,1)S(1)} %slice.20), channel_id=1, source_target_pairs={{0,4},{4,8},{8,12},{12,16},{16,20},{20,24},{24,28},{1,5},{5,9},{9,... | collective-permute-start | bytes 49160 | tf_op jit(solution)/shard_map/ppermute | solution.py:15
  24.2 127.2 %all-gather.2.cloned.1.call-start = ((), (), s32[]{:S(2)}) async-start(), calls=%async_computation.4 | async-start | bytes 3932160 | tf_op jit(solution)/shard_map/all_gather | solution.py:97
  151.4 6.3 %copy-start.3 = (bf16[1,2048,1024]{2,1,0:T(8,128)(2,1)S(1)}, bf16[1,2048,1024]{2,1,0:T(8,128)(2,1)}, u32[]{:S(2)}) copy-start(bf16[1,2048,1024]{2,1,0:T(8,128)(2,1)} %param.21) | copy-start | bytes 12582916
  151.4 6.3 %copy-start.5 = (bf16[8,96,2048]{2,1,0:T(8,128)(2,1)S(1)}, bf16[8,96,2048]{2,1,0:T(8,128)(2,1)}, u32[]{:S(2)}) copy-start(bf16[8,96,2048]{2,1,0:T(8,128)(2,1)} %all-gather.2.cloned.1.call-done) | copy-start | bytes 9437188
  157.7 3.8 %copy-start.4 = (bf16[1,1024,2048]{2,1,0:T(8,128)(2,1)S(1)}, bf16[1,1024,2048]{2,1,0:T(8,128)(2,1)}, u32[]{:S(2)}) copy-start(bf16[1,1024,2048]{2,1,0:T(8,128)(2,1)} %param.23) | copy-start | bytes 12582916
  166.4 5.0 %copy-start.1 = (f32[256,2]{0,1:T(2,128)S(1)}, f32[256,2]{0,1:T(2,128)}, u32[]{:S(2)}) copy-start(f32[256,2]{0,1:T(2,128)} %param.20) | copy-start | bytes 6148
  166.4 76.4 %all-to-all-start.1 = ((bf16[8,96,2048]{2,1,0:T(8,128)(2,1)}), bf16[8,96,2048]{2,1,0:T(8,128)(2,1)}, u32[]{:S(2)}, u32[]{:S(2)}) async-start(bf16[8,96,2048]{2,1,0:T(8,128)(2,1)} %bitcast.56), calls=%async_computation.1 | async-start | bytes 6291456 | tf_op jit(solution)/shard_map/all_to_all | solution.py:108
  171.1 120.5 %reduce-scatter.2.cloned.1.call-start = ((), (), s32[]{:S(2)}) async-start(), calls=%async_computation.5 | async-start | bytes 1310720 | tf_op jit(solution)/shard_map/reduce_scatter | solution.py:112
Sparse Core Ops, SparseCore 0:
  24.3 52.6 all-reduce.1
  109.7 41.6 all-gather.1
  265.7 25.8 reduce-scatter.1
where the time goes:
time: 301 us; the launch traced here: 300 us
  waiting for transfers between devices  185 us (61%)
  local copies, waits for them, and re-layouts  27.1 us (9%)
  blocking collectives  25.5 us (8%)
  other arithmetic  18.3 us (6%)
  matrix products  18.3 us (6%)
  between operations  13.4 us (4%)
  starting transfers between devices  12 us (4%)
    all_to_all x1, waiting for transfers between devices, per_device(): lax.all_to_all(partial_value, 'sp', split_axis=0, concat_axis=0, tiled=True)  71.2 us
    psum x1, waiting for transfers between devices, per_device(): lax.psum(jnp.dot(attended, out_weight, preferred_element_type=jnp.float32...  46.2 us
    all_gather x1, waiting for transfers between devices, per_device(): arrived = lax.all_gather(arrived, 'tp', axis=2, tiled=True)  41.8 us
    reduce_scatter x1, waiting for transfers between devices, per_device(): lax.psum_scatter(jnp.sum(chosen.reshape(row_share * lax.axis_size('tp'),...  26 us
    all_to_all x1, blocking collectives, per_device(): lax.all_to_all(outgoing, 'sp', split_axis=0, concat_axis=0, tiled=True)  25.5 us
    reduce_sum x1, other arithmetic, per_device(): jnp.sum(chosen.reshape(row_share * lax.axis_size('tp'), top_count, chosen...  9.87 us
    gather x1, local copies, waits for them, and re-layouts, per_device(): chosen = returned_flat[targets].astype(jnp.float32) * pair_weights[:, None]  7.56 us
    ppermute x2, starting transfers between devices, shifted(): return lax.ppermute(block, axis, route)  6.98 us
  transfers between devices with their start and end apart: 6, of which 4 were waited for; matrix products, arithmetic and copies ran while one was open for 4% of the time, Pallas kernels for 0%

commit v1 on v0

--- a/solution.py
+++ b/solution.py
@@ -79,8 +79,12 @@
     )
     attended = attended.astype(jnp.bfloat16).reshape(tok_count, local_heads * HEAD_DIM)
     row_share = tok_count // lax.axis_size("tp")
-    projected = lax.psum(
-        jnp.dot(attended, out_weight, preferred_element_type=jnp.float32).astype(jnp.bfloat16), "tp"
+    projected = jnp.sum(
+        lax.all_gather(
+            jnp.dot(attended, out_weight, preferred_element_type=jnp.float32).astype(jnp.bfloat16),
+            "tp",
+        ),
+        axis=0,
     ).astype(jnp.float32)
     stream = (stream_in.astype(jnp.float32) + projected).astype(jnp.bfloat16)
     normed_all = rms_scale(stream, norm_gain)

time: 301 us -> 302 us (level)
  other arithmetic: 18.3 us -> 21.9 us
    psum x1 -> x0, waiting for transfers between devices: 46.2 us -> none  [per_device(): lax.psum(jnp.dot(attended, out_weight, preferred_element_type=jnp.float32...]
    all_gather x0 -> x1, waiting for transfers between devices: none -> 44.9 us  [per_device(): lax.all_gather(jnp.dot(attended, out_weight, preferred_element_type=jnp.f...]
    reduce_sum x0 -> x1, other arithmetic: none -> 4.25 us  [per_device(): jnp.sum(lax.all_gather(jnp.dot(attended, out_weight, preferred_element_ty...]
where the time goes in v1:
time: 302 us; the launch traced here: 301 us
  waiting for transfers between devices  184 us (61%)
  local copies, waits for them, and re-layouts  26.4 us (9%)
  blocking collectives  25.5 us (8%)
  other arithmetic  21.9 us (7%)
  matrix products  18.2 us (6%)
  between operations  13.4 us (4%)
  starting transfers between devices  11.8 us (4%)
    all_to_all x1, waiting for transfers between devices, per_device(): lax.all_to_all(partial_value, 'sp', split_axis=0, concat_axis=0, tiled=True)  71.4 us
    all_gather x1, waiting for transfers between devices, per_device(): lax.all_gather(jnp.dot(attended, out_weight, preferred_element_type=jnp.f...  44.9 us
    all_gather x1, waiting for transfers between devices, per_device(): arrived = lax.all_gather(arrived, 'tp', axis=2, tiled=True)  41.8 us
    reduce_scatter x1, waiting for transfers between devices, per_device(): lax.psum_scatter(jnp.sum(chosen.reshape(row_share * lax.axis_size('tp'),...  26 us
    all_to_all x1, blocking collectives, per_device(): lax.all_to_all(outgoing, 'sp', split_axis=0, concat_axis=0, tiled=True)  25.5 us
    reduce_sum x1, other arithmetic, per_device(): jnp.sum(chosen.reshape(row_share * lax.axis_size('tp'), top_count, chosen...  9.87 us
    gather x1, local copies, waits for them, and re-layouts, per_device(): chosen = returned_flat[targets].astype(jnp.float32) * pair_weights[:, None]  7.56 us
    ppermute x2, starting transfers between devices, shifted(): return lax.ppermute(block, axis, route)  6.98 us
  transfers between devices with their start and end apart: 6, of which 4 were waited for; matrix products, arithmetic and copies ran while one was open for 4% of the time, Pallas kernels for 0%

profile of v1, /device:TPU:0, one launch (start us, length us, event | category | flops | bytes accessed | tf_op | source)
XLA Modules:
  0.0 301.4 jit_solution(3139983673673870034)
XLA Ops:
  6.5 0.0 copy-start
  6.5 0.0 all-gather.6.cloned.1.call-start
  6.5 1.1 constant_dynamic-slice_fusion
  7.6 0.1 copy.28
  7.7 2.4 collective-permute-start.1
  10.1 0.9 constant_dynamic-slice_fusion.1
  11.1 0.1 copy.27
  11.2 4.6 %collective-permute-start = (bf16[128,64]{0,1:T(8,128)(2,1)S(1)}, bf16[128,64]{0,1:T(8,128)(2,1)S(1)}, u32[]{:S(2)}, u32[]{:S(2)}) collective-permute-start(bf16[128,64]{0,1:T(8,128)(2,1)S(1)} %slice.20), channel_id=1, source_target_pairs={{0,4},{4,8},{8,12},{12,16},{16,20},{20,24},{24,28},{1,5},{5,9},{9,... | collective-permute-start | bytes 49160 | tf_op jit(solution)/shard_map/ppermute | solution.py:15
  15.8 0.2 fusion.18
  16.0 1.1 copy.20
  17.1 0.0 collective-permute-done.1
  17.1 0.7 fusion.10
  17.8 0.0 copy-done.3
  17.8 0.1 broadcast_maximum_fusion
  17.9 0.7 fusion.9
  18.5 0.1 exponential_add_fusion
  18.6 0.0 collective-permute-done
  18.6 1.0 fusion.14
  19.6 0.0 copy-start.1
  19.6 0.0 copy-done
  19.6 1.7 convolution_convert_fusion
  21.3 0.0 all-gather.6.cloned.1.call-update
  21.3 0.0 all-gather.4.cloned.1.call-start
  21.4 0.0 copy-done.1
  21.4 0.1 copy.23
  21.5 0.1 eq.29
  21.7 0.1 eq.25
  21.8 1.1 reduce-window.6
  23.0 0.2 slice_reduce_fusion
  23.3 0.1 copy.22
  23.4 0.1 mul.88
  23.6 0.1 fusion.25
  23.7 2.4 scatter_custom_fusion.1
  26.1 2.4 scatter_custom_fusion
  28.6 0.1 broadcast_in_dim.48
  28.7 0.8 dynamic-slice
  29.5 44.9 %all-gather.6.cloned.1.call-done = bf16[1024,2048]{1,0:T(8,128)(2,1)} async-done(((bf16[256,2048]{1,0:T(8,128)(2,1)}), bf16[1024,2048]{1,0:T(8,128)(2,1)}) %all-gather.6.cloned.1.call-update) | async-done | bytes 4194320 | tf_op jit(solution)/shard_map/all_gather | solution.py:83
  74.3 4.3 %reduce_sum.51 = bf16[256,2048]{1,0:T(8,128)(2,1)} reduce(bf16[4,256,2048]{2,1,0:T(8,128)(2,1)} %bitcast.57, bf16[]{:T(256)} %constant.79.clone.1), dimensions={0}, to_apply=%region_2.3 | reduce | flops 1572864 | bytes 5242882 | tf_op jit(solution)/shard_map/reduce_sum | solution.py:82
  78.6 2.0 multiply_reduce_fusion.1
  80.6 0.2 convert_element_type.71
  80.9 0.1 fusion.16
  81.0 3.3 %gather_fusion = bf16[768,512]{1,0:T(8,128)(2,1)} fusion(bf16[256,512]{1,0:T(8,128)(2,1)S(1)} %fusion.16, s32[1024]{0:T(1024)S(1)} %pad_clamp_fusion.1), kind=kCustom, calls=%fused_computation | custom fusion | bytes 1575936 | tf_op jit(solution)/shard_map/gather | solution.py:98
  84.3 1.3 broadcast_select_fusion
  85.7 25.5 %all_to_all.10 = bf16[8,96,512]{2,1,0:T(8,128)(2,1)} all-to-all(bf16[8,96,512]{2,1,0:T(8,128)(2,1)S(1)} %broadcast_select_fusion), channel_id=1, replica_groups=mesh['sp'=8,'tp'=4] {'sp'}, dimensions={0} | all-to-all | bytes 1572864 | tf_op jit(solution)/shard_map/all_to_all | solution.py:100
  111.1 0.0 all-gather.4.cloned.1.call-update
  111.1 41.8 %all-gather.4.cloned.1.call-done = bf16[8,96,2048]{2,1,0:T(8,128)(2,1)} async-done(((bf16[8,96,512]{2,1,0:T(8,128)(2,1)}), bf16[8,96,2048]{2,1,0:T(8,128)(2,1)}) %all-gather.4.cloned.1.call-update) | async-done | bytes 3145744 | tf_op jit(solution)/shard_map/all_gather | solution.py:101
  153.0 6.3 %fusion.2 = f32[768,1024]{1,0:T(8,128)S(1)} fusion(bf16[768,2048]{1,0:T(8,128)(2,1)} %bitcast.66, bf16[1,2048,1024]{2,1,0:T(8,128)(2,1)} %param.22), kind=kOutput, calls=%fused_computation.6 | convolution fusion | flops 3221225472 | bytes 10485760 | tf_op jit(solution)/shard_map/dot_general | solution.py:106
  159.3 0.0 copy-done.4
  159.3 0.0 copy-done.6
  159.3 0.0 copy-start.5
  159.3 3.8 %multiply_convert_fusion = bf16[768,1024]{1,0:T(8,128)(2,1)S(1)} fusion(f32[768,1024]{1,0:T(8,128)S(1)} %fusion.2, bf16[768,2048]{1,0:T(8,128)(2,1)S(1)} %bitcast.67, bf16[1,2048,1024]{2,1,0:T(8,128)(2,1)S(1)} %copy-done.4), kind=kOutput, calls=%fused_computation.13 | convolution fusion | flops 3225944064 | bytes 12058624 | tf_op jit(solution)/shard_map/dot_general | solution.py:105
  163.1 0.0 copy-done.5
  163.1 4.8 %fusion.6 = bf16[768,2048]{1,0:T(8,128)(2,1)} fusion(bf16[768,1024]{1,0:T(8,128)(2,1)S(1)} %multiply_convert_fusion, bf16[1,1024,2048]{2,1,0:T(8,128)(2,1)S(1)} %copy-done.5), kind=kOutput, calls=%fused_computation.11 | convolution fusion | flops 3222798336 | bytes 8912896 | tf_op jit(solution)/shard_map/dot_general | solution.py:108
  167.9 4.7 %all-to-all-start.1 = ((bf16[8,96,2048]{2,1,0:T(8,128)(2,1)}), bf16[8,96,2048]{2,1,0:T(8,128)(2,1)}, u32[]{:S(2)}, u32[]{:S(2)}) async-start(bf16[8,96,2048]{2,1,0:T(8,128)(2,1)} %bitcast.58), calls=%async_computation.1 | async-start | bytes 6291456 | tf_op jit(solution)/shard_map/all_to_all | solution.py:112
  172.7 0.0 reduce-scatter.2.cloned.1.call-start
  172.7 0.0 copy-done.2
  172.7 0.1 copy.25
  172.9 71.4 %all-to-all-done.1 = bf16[8,96,2048]{2,1,0:T(8,128)(2,1)} async-done(((bf16[8,96,2048]{2,1,0:T(8,128)(2,1)}), bf16[8,96,2048]{2,1,0:T(8,128)(2,1)}, u32[]{:S(2)}, u32[]{:S(2)}) %all-to-all-start.1) | async-done | bytes 3145760 | tf_op jit(solution)/shard_map/all_to_all | solution.py:112
  244.3 7.6 %gather_fusion.1 = bf16[512,2048]{1,0:T(8,128)(2,1)} fusion(bf16[768,2048]{1,0:T(8,128)(2,1)} %bitcast.17, s32[1024]{0:T(1024)S(1)} %pad_clamp_fusion), kind=kCustom, calls=%fused_computation.1 | custom fusion | bytes 4196352 | tf_op jit(solution)/shard_map/gather | solution.py:115
  251.8 5.4 %reshape.209 = f32[256,2,2048]{2,1,0:T(2,128)} reshape(bf16[512,2048]{1,0:T(8,128)(2,1)} %gather_fusion.1) | data formatting | bytes 6291456 | tf_op jit(solution)/shard_map/convert_element_type | solution.py:115
  257.3 9.9 %multiply_reduce_fusion = bf16[256,2048]{1,0:T(8,128)(2,1)} fusion(f32[256,2,2048]{2,1,0:T(2,128)} %reshape.209, f32[256,2]{1,0:T(8,128)S(1)} %copy.25), kind=kLoop, calls=%fused_computation.10 | loop fusion | flops 1572864 | bytes 5244928 | tf_op jit(solution)/shard_map/reduce_sum | solution.py:117
  267.1 0.0 reduce-scatter.2.cloned.1.call-update
  267.2 26.0 %reduce-scatter.2.cloned.1.call-done = bf16[64,2048]{1,0:T(8,128)(2,1)} async-done(((bf16[256,2048]{1,0:T(8,128)(2,1)}), bf16[64,2048]{1,0:T(8,128)(2,1)}) %reduce-scatter.2.cloned.1.call-update) | async-done | bytes 262160 | tf_op jit(solution)/shard_map/reduce_scatter | solution.py:116
  293.2 1.7 add_convert_fusion.1
  (21 shorter events, 0.1 us)
Async XLA Ops:
  6.5 13.1 %copy-start = (bf16[512,2048]{1,0:T(8,128)(2,1)S(1)}, bf16[512,2048]{1,0:T(8,128)(2,1)}, u32[]{:S(2)}) copy-start(bf16[512,2048]{1,0:T(8,128)(2,1)} %param.16) | copy-start | bytes 6291460
  6.5 11.2 %copy-start.3 = (f32[8]{0:T(128)S(1)}, f32[8]{0:T(128)}, u32[]{:S(2)}) copy-start(f32[8]{0:T(128)} %param.15) | copy-start | bytes 100
  6.5 67.8 %all-gather.6.cloned.1.call-start = ((), (), s32[]{:S(2)}) async-start(), calls=%async_computation.5 | async-start | bytes 5242880 | tf_op jit(solution)/shard_map/all_gather | solution.py:83
  7.7 9.4 %collective-permute-start.1 = (bf16[128,64]{0,1:T(8,128)(2,1)S(1)}, bf16[128,64]{0,1:T(8,128)(2,1)S(1)}, u32[]{:S(2)}, u32[]{:S(2)}) collective-permute-start(bf16[128,64]{0,1:T(8,128)(2,1)S(1)} %slice.21), channel_id=1, source_target_pairs={{0,4},{4,8},{8,12},{12,16},{16,20},{20,24},{24,28},{1,5},{5,9},{9,... | collective-permute-start | bytes 49160 | tf_op jit(solution)/shard_map/ppermute | solution.py:15
  11.2 7.4 %collective-permute-start = (bf16[128,64]{0,1:T(8,128)(2,1)S(1)}, bf16[128,64]{0,1:T(8,128)(2,1)S(1)}, u32[]{:S(2)}, u32[]{:S(2)}) collective-permute-start(bf16[128,64]{0,1:T(8,128)(2,1)S(1)} %slice.20), channel_id=1, source_target_pairs={{0,4},{4,8},{8,12},{12,16},{16,20},{20,24},{24,28},{1,5},{5,9},{9,... | collective-permute-start | bytes 49160 | tf_op jit(solution)/shard_map/ppermute | solution.py:15
  19.6 1.8 copy-start.1
  21.3 131.6 %all-gather.4.cloned.1.call-start = ((), (), s32[]{:S(2)}) async-start(), calls=%async_computation.3 | async-start | bytes 3932160 | tf_op jit(solution)/shard_map/all_gather | solution.py:101
  153.0 6.3 %copy-start.4 = (bf16[1,2048,1024]{2,1,0:T(8,128)(2,1)S(1)}, bf16[1,2048,1024]{2,1,0:T(8,128)(2,1)}, u32[]{:S(2)}) copy-start(bf16[1,2048,1024]{2,1,0:T(8,128)(2,1)} %param.21) | copy-start | bytes 12582916
  153.0 6.3 %copy-start.6 = (bf16[8,96,2048]{2,1,0:T(8,128)(2,1)S(1)}, bf16[8,96,2048]{2,1,0:T(8,128)(2,1)}, u32[]{:S(2)}) copy-start(bf16[8,96,2048]{2,1,0:T(8,128)(2,1)} %all-gather.4.cloned.1.call-done) | copy-start | bytes 9437188
  159.3 3.8 %copy-start.5 = (bf16[1,1024,2048]{2,1,0:T(8,128)(2,1)S(1)}, bf16[1,1024,2048]{2,1,0:T(8,128)(2,1)}, u32[]{:S(2)}) copy-start(bf16[1,1024,2048]{2,1,0:T(8,128)(2,1)} %param.23) | copy-start | bytes 12582916
  167.9 4.8 %copy-start.2 = (f32[256,2]{0,1:T(2,128)S(1)}, f32[256,2]{0,1:T(2,128)}, u32[]{:S(2)}) copy-start(f32[256,2]{0,1:T(2,128)} %param.20) | copy-start | bytes 6148
  167.9 76.3 %all-to-all-start.1 = ((bf16[8,96,2048]{2,1,0:T(8,128)(2,1)}), bf16[8,96,2048]{2,1,0:T(8,128)(2,1)}, u32[]{:S(2)}, u32[]{:S(2)}) async-start(bf16[8,96,2048]{2,1,0:T(8,128)(2,1)} %bitcast.58), calls=%async_computation.1 | async-start | bytes 6291456 | tf_op jit(solution)/shard_map/all_to_all | solution.py:112
  172.7 120.5 %reduce-scatter.2.cloned.1.call-start = ((), (), s32[]{:S(2)}) async-start(), calls=%async_computation.4 | async-start | bytes 1310720 | tf_op jit(solution)/shard_map/reduce_scatter | solution.py:116
Sparse Core Ops, SparseCore 0:
  21.5 52.8 all-gather.5
  111.3 41.6 all-gather.3
  267.3 25.8 reduce-scatter.1
